TPU v7x, 32 devices: a whole 2x2x4 slice. The times are simulated.
32 devices in a mesh: sp: 4 (over y, x), tp: 8 (over z, core).
Axes of the slice: x: 2, y: 2, z: 4, core: 2. Of those that a mesh axis runs over, the one named last changes fastest.
Arguments:
- queries: bfloat16 [1536, 2048], P('sp', 'tp'), may hold values from -6 to 6
- keys: bfloat16 [1536, 2048], P('sp', 'tp'), may hold values from -6 to 6
- values: bfloat16 [1536, 2048], P('sp', 'tp'), may hold values from -6 to 6
- key_bias: bfloat16 [1536, 32], P('sp', 'tp'), may hold values from -16 to 0
- head_gain: float32 [32, 64], P('tp'), may hold values from 0.1 to 1.9
- out_weight: bfloat16 [2048, 2048], P('tp'), may hold values from -0.125 to 0.125
- residual: bfloat16 [1536, 2048], P(('sp', 'tp')), may hold values from -6 to 6
- norm_gain: float32 [2048], replicated, may hold values from 0.1 to 1.9
- gate_proj: bfloat16 [4, 2048, 7168], P('sp', None, 'tp'), may hold values from -0.125 to 0.125
- up_proj: bfloat16 [4, 2048, 7168], P('sp', None, 'tp'), may hold values from -0.125 to 0.125
- down_proj: bfloat16 [4, 7168, 2048], P('sp', 'tp'), may hold values from -0.0625 to 0.0625
- expert_choice: int32 [1536, 2], P(('sp', 'tp')), may hold values from 0 to 3, all different within a row; in each aligned block of 48 rows (0 to 47, 48 to 95, ...) at most 48 rows name the same one
- expert_weights: float32 [1536, 2], P(('sp', 'tp')), may hold values from 0.2 to 1
Outputs:
- layer_out: bfloat16 [1536, 2048], P(('sp', 'tp'))
Inputs may be any that keep to these rules, and one draw needn't show every extreme that they name: `expert_choice`: in each aligned block of 48 rows (the rows of one device), no expert is named more than 48 times; the two experts of a row differ.
All inputs are finite; a program needn't handle non-finite values.
Results may differ from a plain program's by a relative error of at most 0.019.
Values may be sent and summed in bfloat16 or wider, within the bound.
A program may use at most 128 MiB of HBM per device.

v0:
```python
import jax
import jax.numpy as jnp
from jax import lax
from jax.sharding import PartitionSpec as P

epsilon = 1e-06


def rms_scaled(values_in):
    return values_in * lax.rsqrt(jnp.mean(values_in * values_in, axis=-1, keepdims=True) + epsilon)


def expert_partial(row_block, gate_matrix, up_matrix, down_matrix):
    gate_part = jnp.dot(row_block, gate_matrix, preferred_element_type=jnp.float32)
    up_part = jnp.dot(row_block, up_matrix, preferred_element_type=jnp.float32)
    hidden = (jax.nn.silu(gate_part) * up_part).astype(jnp.bfloat16)
    return jnp.dot(hidden, down_matrix, preferred_element_type=jnp.float32)


def choice_ranks(routes, experts_all):
    flat_routes = routes.reshape(routes.shape[:-2] + (-1,))
    onehot = (flat_routes[..., None] == jnp.arange(experts_all, dtype=jnp.int32)).astype(jnp.int32)
    before = jnp.cumsum(onehot, axis=-2) - onehot
    return jnp.sum(before * onehot, axis=-1).reshape(routes.shape)


def slot_tokens(slot_index, targets, missing):
    flat_slots = slot_index.reshape(-1)
    owners = jnp.arange(flat_slots.shape[0], dtype=jnp.int32) // 2
    matches = flat_slots[None, :] == jnp.arange(targets, dtype=jnp.int32)[:, None]
    owner_found = jnp.sum(jnp.where(matches, owners[None, :], 0), axis=1)
    return jnp.where(jnp.any(matches, axis=1), owner_found, missing)


def on_device(
    queries,
    keys,
    values,
    key_bias,
    head_gain,
    out_weight,
    residual,
    norm_gain,
    gate_proj,
    up_proj,
    down_proj,
    expert_choice,
    expert_weights,
):
    rows_own = queries.shape[0]
    heads_here = head_gain.shape[0]
    head_size = head_gain.shape[1]
    model_width = out_weight.shape[1]
    seq_devices = lax.axis_size("sp")
    head_devices = lax.axis_size("tp")
    own_start = lax.axis_index("sp") * rows_own
    query_pos = own_start + jnp.arange(rows_own, dtype=jnp.int32)
    query_heads = queries.reshape(rows_own, heads_here, head_size)

    def key_block(slot_state, key_rows, value_rows, bias_rows, key_start):
        key_heads = key_rows.reshape(rows_own, heads_here, head_size)
        value_heads = value_rows.reshape(rows_own, heads_here, head_size)
        scores = jnp.einsum(
            "qhd,khd->hqk", query_heads, key_heads, preferred_element_type=jnp.float32
        ) * head_size ** (-0.5)
        scores = scores + bias_rows.astype(jnp.float32).T[:, None, :]
        key_pos = key_start + jnp.arange(rows_own, dtype=jnp.int32)
        earlier = (key_pos[None, :] < query_pos[:, None])[None, :, :]
        log_drops = jnp.where(earlier, jax.nn.log_sigmoid(-scores), 0.0)
        suffix = lax.cumsum(log_drops, axis=2, reverse=True) - log_drops
        within = jnp.where(earlier, jnp.exp(jax.nn.log_sigmoid(scores) + suffix), 0.0).astype(
            jnp.bfloat16
        )
        block_part = jnp.einsum(
            "hqk,khd->qhd", within, value_heads, preferred_element_type=jnp.float32
        )
        block_index = key_start // rows_own
        sums_new = lax.dynamic_update_index_in_dim(
            slot_state[0], block_part.reshape(rows_own, heads_here * head_size), block_index, 0
        )
        totals_new = lax.dynamic_update_index_in_dim(
            slot_state[1], jnp.sum(log_drops, axis=2), block_index, 0
        )
        return (sums_new, totals_new)

    empty_state = (
        jnp.zeros((seq_devices, rows_own, heads_here * head_size), jnp.float32),
        jnp.zeros((seq_devices, heads_here, rows_own), jnp.float32),
    )
    key_piece = lax.all_gather(keys, "sp", axis=0, tiled=True)
    value_piece = lax.all_gather(values, "sp", axis=0, tiled=True)
    bias_piece = lax.all_gather(key_bias, "sp", axis=0, tiled=True)

    def visit(block_count, state_in):
        offset = block_count * rows_own

        def take_rows(array):
            return lax.dynamic_slice_in_dim(array, offset, rows_own, 0)

        def compute(state_now):
            return key_block(
                state_now,
                take_rows(key_piece),
                take_rows(value_piece),
                take_rows(bias_piece),
                offset,
            )

        def keep(state_now):
            return state_now

        return lax.cond(offset <= own_start, compute, keep, state_in)

    block_sums, totals = lax.fori_loop(0, key_piece.shape[0] // rows_own, visit, empty_state)
    carried = jnp.sum(totals, axis=0, keepdims=True) - jnp.cumsum(totals, axis=0)
    factors = jnp.exp(carried).transpose(0, 2, 1)[..., None]
    mixture = jnp.sum(
        factors * block_sums.reshape(seq_devices, rows_own, heads_here, head_size), axis=0
    )
    attended = (
        (rms_scaled(mixture) * head_gain)
        .astype(jnp.bfloat16)
        .reshape(rows_own, heads_here * head_size)
    )
    row_share = rows_own // head_devices
    merged = lax.all_to_all(attended, "tp", split_axis=0, concat_axis=1, tiled=True)
    projected = jnp.dot(
        merged,
        lax.all_gather(out_weight, "tp", axis=0, tiled=True),
        preferred_element_type=jnp.float32,
    )
    stream = (residual.astype(jnp.float32) + projected).astype(jnp.bfloat16)
    normed = (rms_scaled(stream.astype(jnp.float32)) * norm_gain).astype(jnp.bfloat16)
    local_experts = gate_proj.shape[0]
    experts_all = local_experts * seq_devices
    capacity = 4 * rows_own // (head_devices * experts_all)
    own_slots = expert_choice * capacity + choice_ranks(expert_choice, experts_all)
    wanted = slot_tokens(own_slots, experts_all * capacity, row_share)
    outgoing = jnp.take(normed, wanted, axis=0, mode="fill", fill_value=0)
    arrived = lax.all_to_all(
        outgoing.reshape(seq_devices, local_experts, capacity, model_width),
        "sp",
        split_axis=0,
        concat_axis=0,
        tiled=True,
    )
    row_piece = lax.all_gather(arrived, "tp", axis=0, tiled=True)
    count_rows = row_piece.shape[0]
    partials = jnp.stack(
        [
            expert_partial(
                row_piece[:, 0].reshape(-1, model_width), gate_proj[0], up_proj[0], down_proj[0]
            ).reshape(count_rows, capacity, model_width)
        ],
        axis=1,
    )
    summed = lax.psum_scatter(partials.astype(jnp.bfloat16), "tp", scatter_dimension=0, tiled=True)
    returned = lax.all_to_all(summed, "sp", split_axis=0, concat_axis=0, tiled=True).reshape(
        experts_all * capacity, model_width
    )
    picked = jnp.take(returned, own_slots, axis=0).astype(jnp.float32)
    combined = jnp.sum(expert_weights[:, :, None] * picked, axis=1)
    return (stream.astype(jnp.float32) + combined).astype(jnp.bfloat16)


def solution(mesh):
    placed = (
        P("sp", "tp"),
        P("sp", "tp"),
        P("sp", "tp"),
        P("sp", "tp"),
        P("tp", None),
        P("tp", None),
        P(("sp", "tp"), None),
        P(),
        P("sp", None, "tp"),
        P("sp", None, "tp"),
        P("sp", "tp", None),
        P(("sp", "tp"), None),
        P(("sp", "tp"), None),
    )
    return jax.shard_map(
        on_device, mesh=mesh, in_specs=placed, out_specs=P(("sp", "tp"), None), check_vma=False
    )
```

profile of v0, /device:TPU:0, one launch (start us, length us, event | category | flops | bytes accessed | tf_op | source)
XLA Modules:
  0.0 380.5 jit_solution(13210839301603181166)
XLA Ops:
  6.5 0.7 all-gather.3.cloned.1.call-update
  7.3 1.1 copy.81
  8.4 1.1 copy.82
  9.4 1.7 copy.83
  11.2 11.0 %all_gather.17 = bf16[1536,4]{0,1:T(4,128)(2,1)} all-gather(bf16[384,4]{0,1:T(4,128)(2,1)} %param.20), channel_id=1, replica_groups=mesh['sp'=4,'tp'=8] {'sp'}, dimensions={0}, use_global_device_ids=true | all-gather | bytes 15360 | tf_op jit(solution)/shard_map/all_gather | solution.py:92
  22.2 12.4 %all_gather.15 = bf16[1536,256]{0,1:T(8,128)(2,1)} all-gather(bf16[384,256]{0,1:T(8,128)(2,1)S(1)} %copy.81), channel_id=1, replica_groups=mesh['sp'=4,'tp'=8] {'sp'}, dimensions={0}, use_global_device_ids=true | all-gather | bytes 983040 | tf_op jit(solution)/shard_map/all_gather | solution.py:91
  34.5 13.4 %all_gather.16 = bf16[1536,256]{0,1:T(8,128)(2,1)} all-gather(bf16[384,256]{0,1:T(8,128)(2,1)S(1)} %copy.82), channel_id=1, replica_groups=mesh['sp'=4,'tp'=8] {'sp'}, dimensions={0}, use_global_device_ids=true | all-gather | bytes 983040 | tf_op jit(solution)/shard_map/all_gather | solution.py:90
  47.9 1.3 broadcast_in_dim.84
  49.2 0.6 broadcast_in_dim.85
  49.8 28.2 %while.17 = (s32[]{:T(128)}, f32[4,384,256]{1,2,0:T(8,128)}, f32[4,4,384]{2,1,0:T(4,128)}, s32[]{:T(128)}, bf16[1536,256]{0,1:T(8,128)(2,1)}, /*index=5*/bf16[15...) while((s32[]{:T(128)}, f32[4,384,256]{1,2,0:T(8,128)}, ...), condition=%wide.region_6.7_spmd.clone.clone, body=%wide.region_0.6_spmd.clone.clone.sunk | while | flops 246117120 | bytes 38572464 | solution.py:114
  49.8 28.0 %conditional.4 = ((f32[4,384,256]{1,2,0:T(8,128)}, f32[4,4,384]{2,1,0:T(4,128)})) conditional(s32[]{:T(128)} %convert_element_type.76, (f32[4,384,256]{1,2,0:T(8,128)}, f32[4,4,384]{2,1,0:T(4,128)}) %tuple.53, (s32[]{:T(128)}, bf16[1536,256]{0,1:T(8,128)(2,1)}, s32[]{:T(128)}, bf16[1536,256]{0,1:T(8,128)(2,1)}, bf16[384,4,64]{0,2,1:T(8,128)(2,1)}, ...), branch_computations={%region_1.0_spmd, %region_2.5_spmd} | conditional | flops 246117120 | bytes 38570716 | solution.py:112
  49.8 1.1 constant_dynamic-slice_fusion
  50.8 0.7 convert_bitcast_fusion
  51.5 0.1 broadcast_compare_fusion
  51.7 4.3 %fusion.15 = (f32[4,384]{1,0:T(4,128)S(1)}, f32[4,384,384]{1,2,0:T(8,128)S(1)}, f32[4,384,384]{2,1,0:T(8,128)}) fusion(f32[4,384]{1,0:T(4,128)S(1)} %convert_bitcast_fusion, pred[384,384]{0,1:T(8,128)(4,1)S(1)} %broadcast_compare_fusion, bf16[384,4,64]{0,2,1:T(8,128)(2,1)S(1)} %bitcast.92, bf16[384,4,64]{0,2,1:T(8,128)(2,1)} %get-tuple-element.177), kind=kOutput, calls=%fused_computation.33 | convolution fusion | flops 81984000 | bytes 5271552 | tf_op jit(solution)/shard_map/while/body/eval_jaxpr/cond/branch_1_fun/qhd,khd->hqk/dot_general | solution.py:63
  56.0 14.0 %fusion.2 = f32[4,384,3,128]{1,2,3,0:T(4,128)S(1)} fusion(f32[4,384,3,128]{1,3,2,0:T(8,128)S(1)} %bitcast.88), kind=kOutput, calls=%fused_computation.5 | output fusion | flops 74907648 | bytes 4718592 | tf_op jit(solution)/shard_map/reduce-window
  70.1 0.5 broadcast_add_fusion
  70.6 0.2 copy.79
  70.9 1.5 copy-done
  72.3 3.6 fusion.8
  76.0 0.3 fusion.27
  76.3 0.8 constant_dynamic-update-slice_fusion
  77.1 0.6 bitcast_dynamic-update-slice_fusion
  78.0 0.8 reduce_sum.74
  78.7 0.8 fusion.24
  79.5 1.6 fusion.22
  81.1 0.2 copy.84
  81.3 0.1 copy.85
  81.5 0.5 mul.104
  81.9 0.5 mul.105
  82.5 0.7 multiply_convert_fusion.2
  83.2 4.8 %all-to-all-start = ((bf16[8,48,256]{2,1,0:T(8,128)(2,1)}), bf16[8,48,256]{2,1,0:T(8,128)(2,1)S(1)}, u32[]{:S(2)}, u32[]{:S(2)}) async-start(bf16[8,48,256]{2,1,0:T(8,128)(2,1)} %multiply_convert_fusion.2), calls=%async_computation | async-start | bytes 393216 | tf_op jit(solution)/shard_map/all_to_all | solution.py:126
  88.5 0.2 select_reduce_fusion.1
  89.5 6.8 %all-to-all-done = bf16[8,48,256]{2,1,0:T(8,128)(2,1)S(1)} async-done(((bf16[8,48,256]{2,1,0:T(8,128)(2,1)}), bf16[8,48,256]{2,1,0:T(8,128)(2,1)S(1)}, u32[]{:S(2)}, u32[]{:S(2)}) %all-to-all-start) | async-done | bytes 196640 | tf_op jit(solution)/shard_map/all_to_all | solution.py:126
  96.4 5.1 %multiply_reduce_fusion.1 = (f32[48]{0:T(128)S(1)}, f32[48,2048]{1,0:T(8,128)S(1)}) fusion(bf16[48,2048]{1,0:T(8,128)(2,1)S(1)} %bitcast.94, bf16[2048,2048]{1,0:T(8,128)(2,1)} %all-gather.3.cloned.1.call-done, bf16[48,2048]{1,0:T(8,128)(2,1)S(1)} %copy-done.1), kind=kOutput, calls=%fused_computation.54 | convolution fusion | flops 403242944 | bytes 9175232 | tf_op jit(solution)/shard_map/dot_general | solution.py:127
  101.6 1.1 gather_fusion
  102.9 96.4 %all_to_all.26 = bf16[4,1,48,2048]{3,2,1,0:T(8,128)(2,1)} all-to-all(bf16[4,1,48,2048]{3,2,1,0:T(8,128)(2,1)S(1)} %broadcast_select_fusion), channel_id=1, replica_groups=mesh['sp'=4,'tp'=8] {'sp'}, dimensions={0} | all-to-all | bytes 1572864 | tf_op jit(solution)/shard_map/all_to_all | solution.py:140
  199.4 63.5 %all-gather.5.cloned.1.call-done = bf16[32,1,48,2048]{3,2,1,0:T(8,128)(2,1)} async-done(((bf16[4,1,48,2048]{3,2,1,0:T(8,128)(2,1)}), bf16[32,1,48,2048]{3,2,1,0:T(8,128)(2,1)}) %all-gather.5.cloned.1.call-update) | async-done | bytes 6291472 | tf_op jit(solution)/shard_map/all_gather | solution.py:147
  262.9 10.0 %fusion.18 = f32[1536,896]{1,0:T(8,128)S(1)} fusion(bf16[1536,2048]{1,0:T(8,128)(2,1)} %bitcast.101, bf16[1,2048,896]{2,1,0:T(8,128)(2,1)} %param.25), kind=kOutput, calls=%fused_computation.38 | convolution fusion | flops 5637144576 | bytes 15466496 | tf_op jit(solution)/shard_map/dot_general | solution.py:14
  272.9 7.1 %multiply_convert_fusion = bf16[1536,896]{1,0:T(8,128)(2,1)S(1)} fusion(f32[1536,896]{1,0:T(8,128)S(1)} %fusion.18, bf16[1536,2048]{1,0:T(8,128)(2,1)S(1)} %bitcast.102, bf16[1,2048,896]{2,1,0:T(8,128)(2,1)S(1)} %copy-done.7), kind=kOutput, calls=%fused_computation.35 | convolution fusion | flops 5645402112 | bytes 18219008 | tf_op jit(solution)/shard_map/dot_general | solution.py:15
  280.0 8.7 %convert_bitcast_fusion.1 = bf16[32,1,48,2048]{3,2,0,1:T(8,128)(2,1)} fusion(bf16[32,48,896]{2,1,0:T(8,128)(2,1)S(1)} %bitcast.103, bf16[1,896,2048]{2,1,0:T(8,128)(2,1)S(1)} %copy-done.8), kind=kOutput, calls=%fused_computation.34 | convolution fusion | flops 5640290304 | bytes 12713984 | tf_op jit(solution)/shard_map/dot_general | solution.py:17
  288.8 68.5 %reduce-scatter.2.cloned.1.call-done = bf16[4,1,48,2048]{3,2,0,1:T(8,128)(2,1)} async-done(((bf16[32,1,48,2048]{3,2,0,1:T(8,128)(2,1)}), bf16[4,1,48,2048]{3,2,0,1:T(8,128)(2,1)}) %reduce-scatter.2.cloned.1.call-update) | async-done | bytes 786448 | tf_op jit(solution)/shard_map/reduce_scatter | solution.py:157
  357.3 3.7 all-to-all-start.2
  361.5 8.6 %all-to-all-done.2 = bf16[4,1,48,2048]{3,2,1,0:T(8,128)(2,1)S(1)} async-done(((bf16[4,1,48,2048]{3,2,1,0:T(8,128)(2,1)}), bf16[4,1,48,2048]{3,2,1,0:T(8,128)(2,1)S(1)}, u32[]{:S(2)}, u32[]{:S(2)}) %all-to-all-start.2) | async-done | bytes 786464 | tf_op jit(solution)/shard_map/all_to_all | solution.py:158
  370.1 0.8 gather_fusion.1
  370.9 0.3 reshape.183
  371.2 2.1 multiply_reduce_fusion
  373.3 0.7 add_convert_fusion
  (64 shorter events, 2.3 us)
Async XLA Ops:
  6.5 89.9 %all-gather.3.cloned.1.call-start = ((), (), s32[]{:S(2)}) async-start(), calls=%async_computation.4 | async-start | bytes 9437184 | tf_op jit(solution)/shard_map/all_gather | solution.py:129
  70.6 1.7 copy-start
  79.5 2.9 copy-start.4
  81.1 7.0 %copy-start.3 = (s32[48,2]{0,1:T(2,128)S(1)}, s32[48,2]{0,1:T(2,128)}, u32[]{:S(2)}) copy-start(s32[48,2]{0,1:T(2,128)} %param.28) | copy-start | bytes 1156
  81.3 15.1 %copy-start.1 = (bf16[48,2048]{1,0:T(8,128)(2,1)S(1)}, bf16[48,2048]{1,0:T(8,128)(2,1)}, u32[]{:S(2)}) copy-start(bf16[48,2048]{1,0:T(8,128)(2,1)} %param.23) | copy-start | bytes 589828
  83.2 13.1 %all-to-all-start = ((bf16[8,48,256]{2,1,0:T(8,128)(2,1)}), bf16[8,48,256]{2,1,0:T(8,128)(2,1)S(1)}, u32[]{:S(2)}, u32[]{:S(2)}) async-start(bf16[8,48,256]{2,1,0:T(8,128)(2,1)} %multiply_convert_fusion.2), calls=%async_computation | async-start | bytes 393216 | tf_op jit(solution)/shard_map/all_to_all | solution.py:126
  88.0 174.9 %all-gather.5.cloned.1.call-start = ((), (), s32[]{:S(2)}) async-start(), calls=%async_computation.5 | async-start | bytes 7077888 | tf_op jit(solution)/shard_map/all_gather | solution.py:147
  96.4 5.1 %copy-start.2 = (f32[2048]{0:T(1024)S(1)}, f32[2048]{0:T(1024)}, u32[]{:S(2)}) copy-start(f32[2048]{0:T(1024)} %param.24) | copy-start | bytes 24580
  199.3 158.0 %reduce-scatter.2.cloned.1.call-start = ((), (), s32[]{:S(2)}) async-start(), calls=%async_computation.6 | async-start | bytes 7077888 | tf_op jit(solution)/shard_map/reduce_scatter | solution.py:157
  262.9 10.0 %copy-start.6 = (bf16[32,1,48,2048]{3,2,1,0:T(8,128)(2,1)S(1)}, bf16[32,1,48,2048]{3,2,1,0:T(8,128)(2,1)}, u32[]{:S(2)}) copy-start(bf16[32,1,48,2048]{3,2,1,0:T(8,128)(2,1)} %all-gather.5.cloned.1.call-done) | copy-start | bytes 18874372
  262.9 10.0 %copy-start.7 = (bf16[1,2048,896]{2,1,0:T(8,128)(2,1)S(1)}, bf16[1,2048,896]{2,1,0:T(8,128)(2,1)}, u32[]{:S(2)}) copy-start(bf16[1,2048,896]{2,1,0:T(8,128)(2,1)} %param.26) | copy-start | bytes 11010052
  272.9 7.1 %copy-start.8 = (bf16[1,896,2048]{2,1,0:T(8,128)(2,1)S(1)}, bf16[1,896,2048]{2,1,0:T(8,128)(2,1)}, u32[]{:S(2)}) copy-start(bf16[1,896,2048]{2,1,0:T(8,128)(2,1)} %param.27) | copy-start | bytes 11010052
  288.8 72.6 %copy-start.5 = (f32[48,2]{0,1:T(2,128)S(1)}, f32[48,2]{0,1:T(2,128)}, u32[]{:S(2)}) copy-start(f32[48,2]{0,1:T(2,128)} %param.29) | copy-start | bytes 1156
  357.3 12.7 %all-to-all-start.2 = ((bf16[4,1,48,2048]{3,2,1,0:T(8,128)(2,1)}), bf16[4,1,48,2048]{3,2,1,0:T(8,128)(2,1)S(1)}, u32[]{:S(2)}, u32[]{:S(2)}) async-start(bf16[4,1,48,2048]{3,2,1,0:T(8,128)(2,1)} %bitcast.96), calls=%async_computation.3 | async-start | bytes 1572864 | tf_op jit(solution)/shard_map/all_to_all | solution.py:158
Sparse Core Ops, SparseCore 0:
  8.9 84.8 all-gather.2
  199.4 63.4 all-gather.4
  288.9 68.3 reduce-scatter.1
where the time goes:
time: 382 us; the launch traced here: 380 us
  waiting for transfers between devices  148 us (39%)
  blocking collectives  133 us (35%)
  matrix products  35.5 us (9%)
  other arithmetic  26.7 us (7%)
  local copies, waits for them, and re-layouts  14.7 us (4%)
  between operations  13.4 us (4%)
  starting transfers between devices  8.62 us (2%)
    all_to_all x1, blocking collectives, on_device(): lax.all_to_all(outgoing.reshape(seq_devices, local_experts, capacity, mod...  96.4 us
    reduce_scatter x1, waiting for transfers between devices, on_device(): lax.psum_scatter(partials.astype(jnp.bfloat16), 'tp', scatter_dimension=0...  68.5 us
    all_gather x1, waiting for transfers between devices, on_device(): row_piece = lax.all_gather(arrived, 'tp', axis=0, tiled=True)  63.5 us
    another operation x2, other arithmetic  14.1 us
    all_gather x1, blocking collectives, on_device(): key_piece = lax.all_gather(keys, 'sp', axis=0, tiled=True)  13.4 us
    all_gather x1, blocking collectives, on_device(): value_piece = lax.all_gather(values, 'sp', axis=0, tiled=True)  12.4 us
    all_gather x1, blocking collectives, on_device(): bias_piece = lax.all_gather(key_bias, 'sp', axis=0, tiled=True)  11 us
    dot_general x1, matrix products, expert_partial(): jnp.dot(row_block, gate_matrix, preferred_element_type=jnp.float32)  9.96 us
  transfers between devices with their start and end apart: 5, of which 4 were waited for; matrix products, arithmetic and copies ran while one was open for 10% of the time, Pallas kernels for 0%

commit v1 on v0

--- a/solution.py
+++ b/solution.py
@@ -4,6 +4,27 @@
 from jax.sharding import PartitionSpec as P
 
 epsilon = 1e-06
+
+
+def gather_around(x, axis, dim):
+    devices, index, rows = (lax.axis_size(axis), lax.axis_index(axis), x.shape[dim])
+    ahead = [(i, (i + 1) % devices) for i in range(devices)]
+    backward = [(i, (i - 1) % devices) for i in range(devices)]
+    filled = jnp.zeros((*x.shape[:dim], devices * rows, *x.shape[dim + 1 :]), x.dtype)
+    filled = lax.dynamic_update_slice_in_dim(filled, x, index * rows, axis=dim)
+    from_left = from_right = x
+    halfway = devices // 2
+    for step in range(1, halfway + 1):
+        from_left = lax.ppermute(from_left, axis, ahead)
+        filled = lax.dynamic_update_slice_in_dim(
+            filled, from_left, (index - step) % devices * rows, axis=dim
+        )
+        if step < devices - halfway:
+            from_right = lax.ppermute(from_right, axis, backward)
+            filled = lax.dynamic_update_slice_in_dim(
+                filled, from_right, (index + step) % devices * rows, axis=dim
+            )
+    return filled
 
 
 def rms_scaled(values_in):
@@ -144,7 +165,7 @@
         concat_axis=0,
         tiled=True,
     )
-    row_piece = lax.all_gather(arrived, "tp", axis=0, tiled=True)
+    row_piece = gather_around(arrived, "tp", 0)
     count_rows = row_piece.shape[0]
     partials = jnp.stack(
         [

time: 382 us -> 396 us (1.037)
  starting transfers between devices: 8.62 us -> 19.1 us
  loops' own time: 0.31 us -> 8.2 us
  waiting for transfers between devices: 148 us -> 144 us
    all_gather x1 -> x0, waiting for transfers between devices: 63.5 us -> none  [on_device(): row_piece = lax.all_gather(arrived, 'tp', axis=0, tiled=True)]
    ppermute x0 -> x7, waiting for transfers between devices: none -> 61.7 us  [the longest x4 60.1 us: gather_around(): from_left = lax.ppermute(from_left, axis, ahead)]
    ppermute x0 -> x7, starting transfers between devices: none -> 10.7 us  [the longest x3 10.7 us: gather_around(): from_right = lax.ppermute(from_right, axis, backward)]
    another operation x1, loops' own time: 0.2 us -> 8.08 us  [on_device(): lax.fori_loop(0, key_piece.shape[0] // rows_own, visit, empty_state)]
  transfers between devices with their start and end apart: 5 -> 11, of which waited for: 4 -> 8; matrix products, arithmetic and copies ran while one was open for 10% -> 11% of each run, Pallas kernels for 0% -> 0%
where the time goes in v1:
time: 396 us; the launch traced here: 395 us
  waiting for transfers between devices  144 us (36%)
  blocking collectives  133 us (34%)
  matrix products  32.4 us (8%)
  other arithmetic  26.7 us (7%)
  starting transfers between devices  19.1 us (5%)
  local copies, waits for them, and re-layouts  17.5 us (4%)
  between operations  14.1 us (4%)
  loops' own time  8.2 us (2%)
    all_to_all x1, blocking collectives, on_device(): lax.all_to_all(outgoing.reshape(seq_devices, local_experts, capacity, mod...  96.2 us
    reduce_scatter x1, waiting for transfers between devices, on_device(): lax.psum_scatter(partials.astype(jnp.bfloat16), 'tp', scatter_dimension=0...  66.6 us
    ppermute x4, waiting for transfers between devices, gather_around(): from_left = lax.ppermute(from_left, axis, ahead)  60.1 us
    another operation x2, other arithmetic  14.1 us
    all_gather x1, blocking collectives, on_device(): key_piece = lax.all_gather(keys, 'sp', axis=0, tiled=True)  13.4 us
    all_gather x1, blocking collectives, on_device(): value_piece = lax.all_gather(values, 'sp', axis=0, tiled=True)  12.4 us
    all_gather x1, blocking collectives, on_device(): bias_piece = lax.all_gather(key_bias, 'sp', axis=0, tiled=True)  11 us
    ppermute x3, starting transfers between devices, gather_around(): from_right = lax.ppermute(from_right, axis, backward)  10.7 us
  transfers between devices with their start and end apart: 11, of which 8 were waited for; matrix products, arithmetic and copies ran while one was open for 11% of the time, Pallas kernels for 0%

profile of v1, /device:TPU:0, one launch (start us, length us, event | category | flops | bytes accessed | tf_op | source)
XLA Modules:
  0.0 395.4 jit_solution(16256945131953297244)
XLA Ops:
  6.5 0.7 all-gather.2.cloned.1.call-update
  7.3 1.1 copy.81
  8.4 1.1 copy.82
  9.4 1.7 copy.83
  11.2 11.0 %all_gather.14 = bf16[1536,4]{0,1:T(4,128)(2,1)} all-gather(bf16[384,4]{0,1:T(4,128)(2,1)} %param.20), channel_id=1, replica_groups=mesh['sp'=4,'tp'=8] {'sp'}, dimensions={0}, use_global_device_ids=true | all-gather | bytes 15360 | tf_op jit(solution)/shard_map/all_gather | solution.py:113
  22.2 12.4 %all_gather.12 = bf16[1536,256]{0,1:T(8,128)(2,1)} all-gather(bf16[384,256]{0,1:T(8,128)(2,1)S(1)} %copy.81), channel_id=1, replica_groups=mesh['sp'=4,'tp'=8] {'sp'}, dimensions={0}, use_global_device_ids=true | all-gather | bytes 983040 | tf_op jit(solution)/shard_map/all_gather | solution.py:112
  34.5 13.4 %all_gather.13 = bf16[1536,256]{0,1:T(8,128)(2,1)} all-gather(bf16[384,256]{0,1:T(8,128)(2,1)S(1)} %copy.82), channel_id=1, replica_groups=mesh['sp'=4,'tp'=8] {'sp'}, dimensions={0}, use_global_device_ids=true | all-gather | bytes 983040 | tf_op jit(solution)/shard_map/all_gather | solution.py:111
  47.9 1.3 broadcast_in_dim.87
  49.2 0.6 broadcast_in_dim.88
  49.8 36.1 %while.17 = (s32[]{:T(128)}, f32[4,384,256]{1,2,0:T(8,128)}, f32[4,4,384]{2,1,0:T(4,128)}, s32[]{:T(128)}, bf16[1536,256]{0,1:T(8,128)(2,1)}, /*index=5*/bf16[15...) while((s32[]{:T(128)}, f32[4,384,256]{1,2,0:T(8,128)}, ...), condition=%wide.region_6.7_spmd.clone.clone, body=%wide.region_0.6_spmd.clone.clone.sunk | while | flops 246117120 | bytes 38572464 | solution.py:135
  49.8 28.0 %conditional.4 = ((f32[4,384,256]{1,2,0:T(8,128)}, f32[4,4,384]{2,1,0:T(4,128)})) conditional(s32[]{:T(128)} %convert_element_type.76, (f32[4,384,256]{1,2,0:T(8,128)}, f32[4,4,384]{2,1,0:T(4,128)}) %tuple.53, (s32[]{:T(128)}, bf16[1536,256]{0,1:T(8,128)(2,1)}, s32[]{:T(128)}, bf16[1536,256]{0,1:T(8,128)(2,1)}, bf16[384,4,64]{0,2,1:T(8,128)(2,1)}, ...), branch_computations={%region_1.0_spmd, %region_2.5_spmd} | conditional | flops 246117120 | bytes 38570716 | solution.py:133
  49.8 1.1 constant_dynamic-slice_fusion
  50.8 0.7 convert_bitcast_fusion
  51.7 4.3 %fusion.15 = (f32[4,384]{1,0:T(4,128)S(1)}, f32[4,384,384]{1,2,0:T(8,128)S(1)}, f32[4,384,384]{2,1,0:T(8,128)}) fusion(f32[4,384]{1,0:T(4,128)S(1)} %convert_bitcast_fusion, pred[384,384]{0,1:T(8,128)(4,1)S(1)} %broadcast_compare_fusion, bf16[384,4,64]{0,2,1:T(8,128)(2,1)S(1)} %bitcast.96, bf16[384,4,64]{0,2,1:T(8,128)(2,1)} %get-tuple-element.177), kind=kOutput, calls=%fused_computation.33 | convolution fusion | flops 81984000 | bytes 5271552 | tf_op jit(solution)/shard_map/while/body/eval_jaxpr/cond/branch_1_fun/qhd,khd->hqk/dot_general | solution.py:84
  56.0 14.0 %fusion.2 = f32[4,384,3,128]{1,2,3,0:T(4,128)S(1)} fusion(f32[4,384,3,128]{1,3,2,0:T(8,128)S(1)} %bitcast.90), kind=kOutput, calls=%fused_computation.5 | output fusion | flops 74907648 | bytes 4718592 | tf_op jit(solution)/shard_map/reduce-window
  70.1 0.5 broadcast_add_fusion
  70.9 1.5 copy-done
  72.3 3.6 fusion.8
  76.3 0.8 constant_dynamic-update-slice_fusion
  77.1 0.6 bitcast_dynamic-update-slice_fusion
  85.9 0.8 reduce_sum.74
  86.6 0.8 fusion.27
  87.4 1.6 fusion.25
  90.4 0.7 multiply_convert_fusion.2
  91.1 4.8 %all-to-all-start = ((bf16[8,48,256]{2,1,0:T(8,128)(2,1)}), bf16[8,48,256]{2,1,0:T(8,128)(2,1)S(1)}, u32[]{:S(2)}, u32[]{:S(2)}) async-start(bf16[8,48,256]{2,1,0:T(8,128)(2,1)} %multiply_convert_fusion.2), calls=%async_computation | async-start | bytes 393216 | tf_op jit(solution)/shard_map/all_to_all | solution.py:147
  97.4 6.8 %all-to-all-done = bf16[8,48,256]{2,1,0:T(8,128)(2,1)S(1)} async-done(((bf16[8,48,256]{2,1,0:T(8,128)(2,1)}), bf16[8,48,256]{2,1,0:T(8,128)(2,1)S(1)}, u32[]{:S(2)}, u32[]{:S(2)}) %all-to-all-start) | async-done | bytes 196640 | tf_op jit(solution)/shard_map/all_to_all | solution.py:147
  104.3 5.1 %multiply_reduce_fusion.1 = (f32[48]{0:T(128)S(1)}, f32[48,2048]{1,0:T(8,128)S(1)}) fusion(bf16[48,2048]{1,0:T(8,128)(2,1)S(1)} %bitcast.98, bf16[2048,2048]{1,0:T(8,128)(2,1)} %all-gather.2.cloned.1.call-done, bf16[48,2048]{1,0:T(8,128)(2,1)S(1)} %copy-done.3), kind=kOutput, calls=%fused_computation.55 | convolution fusion | flops 403242944 | bytes 9175232 | tf_op jit(solution)/shard_map/dot_general | solution.py:148
  109.5 1.1 gather_fusion
  110.8 96.2 %all_to_all.26 = bf16[4,1,48,2048]{3,2,1,0:T(8,128)(2,1)S(1)} all-to-all(bf16[4,1,48,2048]{3,2,1,0:T(8,128)(2,1)S(1)} %broadcast_select_fusion), channel_id=1, replica_groups=mesh['sp'=4,'tp'=8] {'sp'}, dimensions={0} | all-to-all | bytes 1572864 | tf_op jit(solution)/shard_map/all_to_all | solution.py:161
  207.0 3.5 collective-permute-start.1
  210.5 17.1 %collective-permute-done = bf16[4,1,48,2048]{3,2,1,0:T(8,128)(2,1)S(1)} collective-permute-done((bf16[4,1,48,2048]{3,2,1,0:T(8,128)(2,1)S(1)}, bf16[4,1,48,2048]{3,2,1,0:T(8,128)(2,1)S(1)}, u32[]{:S(2)}, u32[]{:S(2)}) %collective-permute-start) | collective-permute-done | bytes 786464 | tf_op jit(solution)/shard_map/ppermute | solution.py:18
  227.6 3.5 collective-permute-start.3
  231.2 17.9 %collective-permute-done.2 = bf16[4,1,48,2048]{3,2,1,0:T(8,128)(2,1)S(1)} collective-permute-done((bf16[4,1,48,2048]{3,2,1,0:T(8,128)(2,1)S(1)}, bf16[4,1,48,2048]{3,2,1,0:T(8,128)(2,1)S(1)}, u32[]{:S(2)}, u32[]{:S(2)}) %collective-permute-start.2) | collective-permute-done | bytes 786464 | tf_op jit(solution)/shard_map/ppermute | solution.py:18
  249.0 0.8 broadcast_in_dim.90
  250.3 3.6 collective-permute-start.5
  253.9 1.2 constant_dynamic-update-slice_fusion.5
  255.1 13.9 %collective-permute-done.4 = bf16[4,1,48,2048]{3,2,1,0:T(8,128)(2,1)S(1)} collective-permute-done((bf16[4,1,48,2048]{3,2,1,0:T(8,128)(2,1)S(1)}, bf16[4,1,48,2048]{3,2,1,0:T(8,128)(2,1)S(1)}, u32[]{:S(2)}, u32[]{:S(2)}) %collective-permute-start.4) | collective-permute-done | bytes 786464 | tf_op jit(solution)/shard_map/ppermute | solution.py:18
  269.3 1.6 collective-permute-done.5
  270.9 11.2 %collective-permute-done.6 = bf16[4,1,48,2048]{3,2,1,0:T(8,128)(2,1)S(1)} collective-permute-done((bf16[4,1,48,2048]{3,2,1,0:T(8,128)(2,1)S(1)}, bf16[4,1,48,2048]{3,2,1,0:T(8,128)(2,1)S(1)}, u32[]{:S(2)}, u32[]{:S(2)}) %collective-permute-start.6) | collective-permute-done | bytes 786464 | tf_op jit(solution)/shard_map/ppermute | solution.py:18
  282.3 6.7 %fusion.21 = f32[1536,896]{1,0:T(8,128)S(1)} fusion(bf16[1536,2048]{1,0:T(8,128)(2,1)S(1)} %bitcast.94, bf16[1,2048,896]{2,1,0:T(8,128)(2,1)S(1)} %copy-done.8), kind=kOutput, calls=%fused_computation.39 | convolution fusion | flops 5637144576 | bytes 15466496 | tf_op jit(solution)/shard_map/dot_general | solution.py:35
  289.0 7.3 %multiply_convert_fusion = bf16[1536,896]{1,0:T(8,128)(2,1)S(1)} fusion(f32[1536,896]{1,0:T(8,128)S(1)} %fusion.21, bf16[1536,2048]{1,0:T(8,128)(2,1)S(1)} %bitcast.95, bf16[1,2048,896]{2,1,0:T(8,128)(2,1)S(1)} %copy-done.9), kind=kOutput, calls=%fused_computation.35 | convolution fusion | flops 5645402112 | bytes 18219008 | tf_op jit(solution)/shard_map/dot_general | solution.py:36
  296.3 8.7 %convert_bitcast_fusion.1 = bf16[32,1,48,2048]{3,2,0,1:T(8,128)(2,1)} fusion(bf16[32,48,896]{2,1,0:T(8,128)(2,1)S(1)} %bitcast.105, bf16[1,896,2048]{2,1,0:T(8,128)(2,1)S(1)} %copy-done.10), kind=kOutput, calls=%fused_computation.34 | convolution fusion | flops 5640290304 | bytes 12713984 | tf_op jit(solution)/shard_map/dot_general | solution.py:38
  305.1 66.6 %reduce-scatter.2.cloned.1.call-done = bf16[4,1,48,2048]{3,2,0,1:T(8,128)(2,1)} async-done(((bf16[32,1,48,2048]{3,2,0,1:T(8,128)(2,1)}), bf16[4,1,48,2048]{3,2,0,1:T(8,128)(2,1)}) %reduce-scatter.2.cloned.1.call-update) | async-done | bytes 786448 | tf_op jit(solution)/shard_map/reduce_scatter | solution.py:178
  371.6 3.6 all-to-all-start.2
  375.7 8.7 %all-to-all-done.2 = bf16[4,1,48,2048]{3,2,1,0:T(8,128)(2,1)S(1)} async-done(((bf16[4,1,48,2048]{3,2,1,0:T(8,128)(2,1)}), bf16[4,1,48,2048]{3,2,1,0:T(8,128)(2,1)S(1)}, u32[]{:S(2)}, u32[]{:S(2)}) %all-to-all-start.2) | async-done | bytes 786464 | tf_op jit(solution)/shard_map/all_to_all | solution.py:179
  384.4 0.8 gather_fusion.1
  385.5 2.0 multiply_reduce_fusion
  387.5 0.7 add_convert_fusion
  (88 shorter events, 5.4 us)
Async XLA Ops:
  6.5 97.7 %all-gather.2.cloned.1.call-start = ((), (), s32[]{:S(2)}) async-start(), calls=%async_computation.4 | async-start | bytes 9437184 | tf_op jit(solution)/shard_map/all_gather | solution.py:150
  70.6 1.7 copy-start
  85.8 4.5 %copy-start.6 = (f32[4,64]{1,0:T(4,128)S(1)}, f32[4,64]{1,0:T(4,128)}, u32[]{:S(2)}) copy-start(f32[4,64]{1,0:T(4,128)} %param.21) | copy-start | bytes 3076
  87.4 8.6 %copy-start.5 = (s32[48,2]{0,1:T(2,128)S(1)}, s32[48,2]{0,1:T(2,128)}, u32[]{:S(2)}) copy-start(s32[48,2]{0,1:T(2,128)} %param.28) | copy-start | bytes 1156
  89.0 15.3 %copy-start.3 = (bf16[48,2048]{1,0:T(8,128)(2,1)S(1)}, bf16[48,2048]{1,0:T(8,128)(2,1)}, u32[]{:S(2)}) copy-start(bf16[48,2048]{1,0:T(8,128)(2,1)} %param.23) | copy-start | bytes 589828
  91.1 13.1 %all-to-all-start = ((bf16[8,48,256]{2,1,0:T(8,128)(2,1)}), bf16[8,48,256]{2,1,0:T(8,128)(2,1)S(1)}, u32[]{:S(2)}, u32[]{:S(2)}) async-start(bf16[8,48,256]{2,1,0:T(8,128)(2,1)} %multiply_convert_fusion.2), calls=%async_computation | async-start | bytes 393216 | tf_op jit(solution)/shard_map/all_to_all | solution.py:147
  95.9 275.7 %reduce-scatter.2.cloned.1.call-start = ((), (), s32[]{:S(2)}) async-start(), calls=%async_computation.5 | async-start | bytes 7077888 | tf_op jit(solution)/shard_map/reduce_scatter | solution.py:178
  104.3 5.1 %copy-start.4 = (f32[2048]{0:T(1024)S(1)}, f32[2048]{0:T(1024)}, u32[]{:S(2)}) copy-start(f32[2048]{0:T(1024)} %param.24) | copy-start | bytes 24580
  207.0 20.6 %collective-permute-start = (bf16[4,1,48,2048]{3,2,1,0:T(8,128)(2,1)S(1)}, bf16[4,1,48,2048]{3,2,1,0:T(8,128)(2,1)S(1)}, u32[]{:S(2)}, u32[]{:S(2)}) collective-permute-start(bf16[4,1,48,2048]{3,2,1,0:T(8,128)(2,1)S(1)} %all_to_all.26), channel_id=1, source_target_pairs={{0,1},{1,2},{2,3},{3,4},{4,5},{5,6},{6,7},{7,0},{8,9},{9,10},{10,1... | collective-permute-start | bytes 2359304 | tf_op jit(solution)/shard_map/ppermute | solution.py:18
  207.0 20.6 %collective-permute-start.1 = (bf16[4,1,48,2048]{3,2,1,0:T(8,128)(2,1)S(1)}, bf16[4,1,48,2048]{3,2,1,0:T(8,128)(2,1)}, u32[]{:S(2)}, u32[]{:S(2)}) collective-permute-start(bf16[4,1,48,2048]{3,2,1,0:T(8,128)(2,1)S(1)} %all_to_all.26), channel_id=1, source_target_pairs={{0,7},{1,0},{2,1},{3,2},{4,3},{5,4},{6,5},{7,6},{8,15},{9,8},{10,9... | collective-permute-start | bytes 2359304 | tf_op jit(solution)/shard_map/ppermute | solution.py:23
  227.6 3.6 copy-start.1
  227.6 21.4 %collective-permute-start.2 = (bf16[4,1,48,2048]{3,2,1,0:T(8,128)(2,1)S(1)}, bf16[4,1,48,2048]{3,2,1,0:T(8,128)(2,1)S(1)}, u32[]{:S(2)}, u32[]{:S(2)}) collective-permute-start(bf16[4,1,48,2048]{3,2,1,0:T(8,128)(2,1)S(1)} %collective-permute-done), channel_id=1, source_target_pairs={{0,1},{1,2},{2,3},{3,4},{4,5},{5,6},{6,7},{7,0},{8,9},{9,10},{10,1... | collective-permute-start | bytes 2359304 | tf_op jit(solution)/shard_map/ppermute | solution.py:18
  227.6 22.6 %collective-permute-start.3 = (bf16[4,1,48,2048]{3,2,1,0:T(8,128)(2,1)}, bf16[4,1,48,2048]{3,2,1,0:T(8,128)(2,1)S(1)}, u32[]{:S(2)}, u32[]{:S(2)}) collective-permute-start(bf16[4,1,48,2048]{3,2,1,0:T(8,128)(2,1)} %collective-permute-done.1), channel_id=1, source_target_pairs={{0,7},{1,0},{2,1},{3,2},{4,3},{5,4},{6,5},{7,6},{8,15},{9,8},{10,9... | collective-permute-start | bytes 2359304 | tf_op jit(solution)/shard_map/ppermute | solution.py:23
  249.0 19.9 %collective-permute-start.4 = (bf16[4,1,48,2048]{3,2,1,0:T(8,128)(2,1)S(1)}, bf16[4,1,48,2048]{3,2,1,0:T(8,128)(2,1)S(1)}, u32[]{:S(2)}, u32[]{:S(2)}) collective-permute-start(bf16[4,1,48,2048]{3,2,1,0:T(8,128)(2,1)S(1)} %collective-permute-done.2), channel_id=1, source_target_pairs={{0,1},{1,2},{2,3},{3,4},{4,5},{5,6},{6,7},{7,0},{8,9},{9,10},{10,1... | collective-permute-start | bytes 2359304 | tf_op jit(solution)/shard_map/ppermute | solution.py:18
  249.0 1.1 copy-start.2
  250.3 20.6 %collective-permute-start.5 = (bf16[4,1,48,2048]{3,2,1,0:T(8,128)(2,1)S(1)}, bf16[4,1,48,2048]{3,2,1,0:T(8,128)(2,1)S(1)}, u32[]{:S(2)}, u32[]{:S(2)}) collective-permute-start(bf16[4,1,48,2048]{3,2,1,0:T(8,128)(2,1)S(1)} %collective-permute-done.3), channel_id=1, source_target_pairs={{0,7},{1,0},{2,1},{3,2},{4,3},{5,4},{6,5},{7,6},{8,15},{9,8},{10,9... | collective-permute-start | bytes 2359304 | tf_op jit(solution)/shard_map/ppermute | solution.py:23
  269.0 13.2 %collective-permute-start.6 = (bf16[4,1,48,2048]{3,2,1,0:T(8,128)(2,1)S(1)}, bf16[4,1,48,2048]{3,2,1,0:T(8,128)(2,1)S(1)}, u32[]{:S(2)}, u32[]{:S(2)}) collective-permute-start(bf16[4,1,48,2048]{3,2,1,0:T(8,128)(2,1)S(1)} %collective-permute-done.4), channel_id=1, source_target_pairs={{0,1},{1,2},{2,3},{3,4},{4,5},{5,6},{6,7},{7,0},{8,9},{9,10},{10,1... | collective-permute-start | bytes 2359304 | tf_op jit(solution)/shard_map/ppermute | solution.py:18
  269.1 13.2 %copy-start.8 = (bf16[1,2048,896]{2,1,0:T(8,128)(2,1)S(1)}, bf16[1,2048,896]{2,1,0:T(8,128)(2,1)}, u32[]{:S(2)}) copy-start(bf16[1,2048,896]{2,1,0:T(8,128)(2,1)} %param.25) | copy-start | bytes 11010052
  282.3 6.8 %copy-start.9 = (bf16[1,2048,896]{2,1,0:T(8,128)(2,1)S(1)}, bf16[1,2048,896]{2,1,0:T(8,128)(2,1)}, u32[]{:S(2)}) copy-start(bf16[1,2048,896]{2,1,0:T(8,128)(2,1)} %param.26) | copy-start | bytes 11010052
  289.0 7.3 %copy-start.10 = (bf16[1,896,2048]{2,1,0:T(8,128)(2,1)S(1)}, bf16[1,896,2048]{2,1,0:T(8,128)(2,1)}, u32[]{:S(2)}) copy-start(bf16[1,896,2048]{2,1,0:T(8,128)(2,1)} %param.27) | copy-start | bytes 11010052
  305.0 70.6 %copy-start.7 = (f32[48,2]{0,1:T(2,128)S(1)}, f32[48,2]{0,1:T(2,128)}, u32[]{:S(2)}) copy-start(f32[48,2]{0,1:T(2,128)} %param.29) | copy-start | bytes 1156
  371.6 12.7 %all-to-all-start.2 = ((bf16[4,1,48,2048]{3,2,1,0:T(8,128)(2,1)}), bf16[4,1,48,2048]{3,2,1,0:T(8,128)(2,1)S(1)}, u32[]{:S(2)}, u32[]{:S(2)}) async-start(bf16[4,1,48,2048]{3,2,1,0:T(8,128)(2,1)} %bitcast.100), calls=%async_computation.3 | async-start | bytes 1572864 | tf_op jit(solution)/shard_map/all_to_all | solution.py:179
Sparse Core Ops, SparseCore 0:
  8.9 84.7 all-gather.1
  305.2 66.4 reduce-scatter.1
